TPU v7x, 32 devices: a whole 2x2x4 slice. The times are simulated.
32 devices in a mesh: grp: 2 (over x), ep: 16 (over z, y, core).
Axes of the slice: x: 2, y: 2, z: 4, core: 2. Of those that a mesh axis runs over, the one named last changes fastest.
Arguments:
- tokens: bfloat16 [128, 2048], P(('grp', 'ep')), parts along dimension 0, may hold values from -6 to 6
- lengths: int32 [128], P(('grp', 'ep')), parts along dimension 0, may hold values from 128 to 1024, as said below
- cache_key: bfloat16 [128, 1024, 256], P(('grp', 'ep')), parts along dimension 0, may hold values from -6 to 6
- cache_value: bfloat16 [128, 1024, 256], P(('grp', 'ep')), parts along dimension 0, may hold values from -6 to 6
- routes: int32 [128, 2], P(('grp', 'ep')), parts along dimension 0, may hold values from 0 to 3, all different within a row
- route_logits: float32 [128, 2], P(('grp', 'ep')), parts along dimension 0, may hold values from -6 to 6
- mix_gain: float32 [2048], replicated, may hold values from 0.1 to 1.9
- query_gain: float32 [64], replicated, may hold values from 0.1 to 1.9
- key_gain: float32 [64], replicated, may hold values from 0.1 to 1.9
- head_bias: float32 [16], replicated, may hold values from -9 to -3.5
- w_query: bfloat16 [2048, 1024], P('ep'), may hold values from -0.125 to 0.125
- w_key: bfloat16 [2048, 256], P('ep'), may hold values from -0.125 to 0.125
- w_value: bfloat16 [2048, 256], P('ep'), may hold values from -0.125 to 0.125
- w_out: bfloat16 [1024, 2048], P(None, 'ep'), may hold values from -0.1875 to 0.1875
- ffn_gain: float32 [2048], replicated, may hold values from 0.1 to 1.9
- w_gate: bfloat16 [2048, 28672], P(None, 'ep'), may hold values from -0.125 to 0.125
- w_up: bfloat16 [2048, 28672], P(None, 'ep'), may hold values from -0.125 to 0.125
- w_down: bfloat16 [28672, 2048], P('ep'), may hold values from -0.0625 to 0.0625
Outputs:
- output: bfloat16 [128, 2048], P(('grp', 'ep')), parts along dimension 0
- new_key: bfloat16 [128, 256], P(('grp', 'ep')), parts along dimension 0
- new_value: bfloat16 [128, 256], P(('grp', 'ep')), parts along dimension 0
There are 2 independent parts, one for each index of `grp`. A program takes and returns all parts, laid end to end along the dimension named above; an argument that names none is the same for every part. Nothing has to cross between parts.
Inputs may be any that keep to these rules, and one draw needn't show every extreme that they name: `lengths`: some sequence has all 1024 positions live.
All inputs are finite; a program needn't handle non-finite values.
Results may differ from a plain program's by a relative error of at most 0.0085.
Values may be sent and summed in bfloat16 or wider, within the bound.
No kernel may reach another device: no remote copies, remote signals or barrier semaphores. Data moves between devices by JAX's collectives and lax.ppermute only.
A program may use at most 128 MiB of HBM per device.

v0:
```python
import jax
import jax.numpy as jnp
from jax import lax
from jax.sharding import PartitionSpec as P

HEADS = 16
KV_HEADS = 4
HEAD_DIM = 64
FF = 7168
EXPERTS = 4
EPSILON = 1e-06


def rms_scaled(values, gain):
    return values * lax.rsqrt(jnp.mean(values * values, axis=-1, keepdims=True) + EPSILON) * gain


def route_weights(routes, route_logits):
    experts_iota = jnp.arange(EXPERTS, dtype=jnp.int32)[None, :]
    first_share = jax.nn.sigmoid(route_logits[:, 0:1] - route_logits[:, 1:2])
    second_share = jax.nn.sigmoid(route_logits[:, 1:2] - route_logits[:, 0:1])
    return jnp.where(routes[:, 0:1] == experts_iota, first_share, 0.0) + jnp.where(
        routes[:, 1:2] == experts_iota, second_share, 0.0
    )


def stick_attend(queries, lengths, cache_key, cache_value, query_gain, head_bias):
    batch_rows = queries.shape[0]
    cache_len = cache_key.shape[1]
    group_size = HEADS // KV_HEADS
    normed_query = rms_scaled(queries.reshape(batch_rows, HEADS, HEAD_DIM), query_gain).astype(
        jnp.bfloat16
    )
    normed_query = normed_query.reshape(batch_rows, KV_HEADS, group_size, HEAD_DIM)
    key_heads = cache_key.reshape(batch_rows, cache_len, KV_HEADS, HEAD_DIM)
    value_heads = cache_value.reshape(batch_rows, cache_len, KV_HEADS, HEAD_DIM)
    scores = jnp.einsum(
        "bkgd,blkd->bkgl", normed_query, key_heads, preferred_element_type=jnp.float32
    ) * HEAD_DIM ** (-0.5)
    scores = scores + head_bias.reshape(KV_HEADS, group_size)[None, :, :, None]
    live_mask = (
        jnp.arange(cache_len, dtype=jnp.int32)[None, None, None, :] < lengths[:, None, None, None]
    )
    remain = jnp.where(live_mask, jax.nn.log_sigmoid(-scores), 0.0)
    after_sum = lax.cumsum(remain, axis=3, reverse=True) - remain
    weights = jnp.where(live_mask, jnp.exp(jax.nn.log_sigmoid(scores) + after_sum), 0.0).astype(
        jnp.bfloat16
    )
    attended = jnp.einsum(
        "bkgl,blkd->bkgd", weights, value_heads, preferred_element_type=jnp.float32
    )
    return attended.reshape(batch_rows, HEADS * HEAD_DIM).astype(jnp.bfloat16)


def local(
    tokens,
    lengths,
    cache_key,
    cache_value,
    routes,
    route_logits,
    mix_gain,
    query_gain,
    key_gain,
    head_bias,
    w_query,
    w_key,
    w_value,
    w_out,
    ffn_gain,
    w_gate,
    w_up,
    w_down,
):
    token_rows = tokens.shape[0]
    key_width = w_key.shape[1]
    as_float = tokens.astype(jnp.float32)
    normed = rms_scaled(as_float, mix_gain).astype(jnp.bfloat16)
    pieces = (
        lax.all_gather(w_query, "ep", axis=0, tiled=True),
        lax.all_gather(w_key, "ep", axis=0, tiled=True),
        lax.all_gather(w_value, "ep", axis=0, tiled=True),
    )
    queries, fresh_key, fresh_value = tuple(
        (jnp.dot(normed, weight, preferred_element_type=jnp.float32) for weight in pieces)
    )
    new_key = rms_scaled(fresh_key.reshape(token_rows, KV_HEADS, HEAD_DIM), key_gain)
    new_key = new_key.reshape(token_rows, key_width).astype(jnp.bfloat16)
    new_value = fresh_value.astype(jnp.bfloat16)
    attended = stick_attend(queries, lengths, cache_key, cache_value, query_gain, head_bias)
    mixed = as_float + jnp.dot(
        attended,
        lax.all_gather(w_out, "ep", axis=1, tiled=True),
        preferred_element_type=jnp.float32,
    )
    expert_in = rms_scaled(mixed, ffn_gain).astype(jnp.bfloat16)
    every_gate = lax.all_gather(route_weights(routes, route_logits), "ep", axis=0, tiled=True)
    ff_share = w_gate.shape[1]
    my_expert = lax.axis_index("ep") // (FF // ff_share)
    my_gate = lax.dynamic_slice_in_dim(every_gate, my_expert, 1, 1)
    input_rows = lax.all_gather(expert_in, "ep", axis=0, tiled=True)
    gate_value = jnp.dot(input_rows, w_gate, preferred_element_type=jnp.float32)
    up_value = jnp.dot(input_rows, w_up, preferred_element_type=jnp.float32)
    hidden = (jax.nn.silu(gate_value) * up_value * my_gate).astype(jnp.bfloat16)
    expert_sum = lax.psum_scatter(
        jnp.dot(hidden, w_down, preferred_element_type=jnp.float32),
        "ep",
        scatter_dimension=0,
        tiled=True,
    )
    return ((mixed + expert_sum).astype(jnp.bfloat16), new_key, new_value)


def solution(mesh):
    return jax.shard_map(
        local,
        mesh=mesh,
        in_specs=(
            P(("grp", "ep"), None),
            P(("grp", "ep")),
            P(("grp", "ep"), None, None),
            P(("grp", "ep"), None, None),
            P(("grp", "ep"), None),
            P(("grp", "ep"), None),
            P(),
            P(),
            P(),
            P(),
            P("ep", None),
            P("ep", None),
            P("ep", None),
            P(None, "ep"),
            P(),
            P(None, "ep"),
            P(None, "ep"),
            P("ep", None),
        ),
        out_specs=(P(("grp", "ep"), None), P(("grp", "ep"), None), P(("grp", "ep"), None)),
        check_vma=False,
    )
```

profile of v0, /device:TPU:0, one launch (start us, length us, event | category | flops | bytes accessed | tf_op | source)
XLA Modules:
  0.0 323.6 jit_solution(14233699592130676212)
XLA Ops:
  7.2 0.7 all-gather.11.cloned.1.call-update
  8.0 0.7 all-gather.7.cloned.1.call-update
  10.1 0.8 slice_bitcast_fusion.1
  10.8 0.8 divide_bitcast_fusion.1
  11.6 23.2 %all-gather.1 = f32[16,4,4]{2,1,0:T(4,128)S(1)} all-gather(f32[1,4,4]{2,1,0:T(4,128)S(1)} %add_bitcast_fusion), channel_id=1, replica_groups=mesh['grp'=2,'ep'=16] {'ep'}, dimensions={0}, use_global_device_ids=true | all-gather | bytes 1088 | tf_op jit(solution)/shard_map/all_gather | solution.py:97
  35.0 0.9 fusion.21
  35.9 0.7 iota_compare_fusion
  36.6 4.0 %copy.27 = bf16[4,1024,256]{1,2,0:T(8,128)(2,1)} copy(bf16[4,1024,256]{2,1,0:T(8,128)(2,1)} %param.20) | data formatting | bytes 4194304 | tf_op args[2]
  40.7 2.6 copy.28
  44.6 6.3 %all-gather.11.cloned.1.call-done = bf16[2048,256]{1,0:T(8,128)(2,1)} async-done(((bf16[128,256]{1,0:T(8,128)(2,1)}), bf16[2048,256]{1,0:T(8,128)(2,1)}) %all-gather.11.cloned.1.call-update) | async-done | bytes 1048592 | tf_op jit(solution)/shard_map/all_gather | solution.py:81
  50.8 1.5 fusion.37
  52.7 49.7 %all-gather.7.cloned.1.call-done = bf16[2048,1024]{1,0:T(8,128)(2,1)} async-done(((bf16[128,1024]{1,0:T(8,128)(2,1)}), bf16[2048,1024]{1,0:T(8,128)(2,1)}) %all-gather.7.cloned.1.call-update) | async-done | bytes 4194320 | tf_op jit(solution)/shard_map/all_gather | solution.py:80
  102.4 2.9 fusion.36
  105.6 2.2 fusion.15
  108.0 79.2 %reduce-window.6 = f32[4,4,4,8,128]{4,3,2,1,0:T(8,128)S(1)} reduce-window(f32[4,4,4,8,128]{4,3,2,1,0:T(8,128)S(1)} %reshape.103, f32[]{:T(128)} %constant.36.clone.1), window={size=1x1x1x1x128 pad=0_0x0_0x0_0x0_0x0_127}, to_apply=%region_2.0 | reduce-window | flops 8323072 | bytes 524292 | tf_op jit(solution)/shard_map/reduce-window
  187.4 2.8 reduce-window.9
  190.6 0.9 convolution_convert_fusion
  191.6 3.0 multiply_reduce_fusion
  194.7 19.6 %all-gather = bf16[16,4,2048]{2,1,0:T(4,128)(2,1)S(1)} all-gather(bf16[1,4,2048]{2,1,0:T(4,128)(2,1)S(1)} %fusion.25), channel_id=1, replica_groups=mesh['grp'=2,'ep'=16] {'ep'}, dimensions={0}, use_global_device_ids=true | all-gather | bytes 278528 | tf_op jit(solution)/shard_map/all_gather | solution.py:101
  214.4 4.4 %fusion.38 = f32[64,1792]{1,0:T(8,128)S(1)} fusion(bf16[64,2048]{1,0:T(8,128)(2,1)S(1)} %reshape.107, bf16[2048,1792]{1,0:T(8,128)(2,1)} %param.33), kind=kOutput, calls=%fused_computation.62 | convolution fusion | flops 469762048 | bytes 8060928 | tf_op jit(solution)/shard_map/dot_general | solution.py:102
  218.8 8.7 %fusion.3 = f32[64,2048]{1,0:T(8,128)} fusion(bf16[1792,2048]{1,0:T(8,128)(2,1)} %param.35, bf16[64,2048]{1,0:T(8,128)(2,1)S(1)} %reshape.107, bf16[2048,1792]{1,0:T(8,128)(2,1)} %param.34, f32[64,1792]{1,0:T(8,128)S(1)} %fusion.38, f32[64]{0:T(128)S(1)} %bitcast.34), kind=kOutput, calls=%fused_computation.8 | convolution fusion | flops 940326912 | bytes 15925504 | tf_op jit(solution)/shard_map/dot_general | solution.py:106
  228.1 2.1 convolution_convert_fusion.1
  230.2 85.5 %all-reduce.3.cloned.1.call-done = f32[64,2048]{1,0:T(8,128)} async-done(((f32[64,2048]{1,0:T(8,128)}), f32[64,2048]{1,0:T(8,128)}) %all-reduce.3.cloned.1.call-update) | async-done | bytes 524304
  315.7 1.5 fusion.24
  (56 shorter events, 4.6 us)
Async XLA Ops:
  7.2 33.4 %copy-start.5 = (f32[16]{0:T(128)S(1)}, f32[16]{0:T(128)}, u32[]{:S(2)}) copy-start(f32[16]{0:T(128)} %param.27) | copy-start | bytes 196
  7.2 33.5 %copy-start = (bf16[4,1024,256]{2,1,0:T(8,128)(2,1)S(1)}, bf16[4,1024,256]{2,1,0:T(8,128)(2,1)}, u32[]{:S(2)}) copy-start(bf16[4,1024,256]{2,1,0:T(8,128)(2,1)} %param.21) | copy-start | bytes 6291460
  7.2 43.6 %all-gather.11.cloned.1.call-start = ((), (), s32[]{:S(2)}) async-start(), calls=%async_computation.2 | async-start | bytes 1114112 | tf_op jit(solution)/shard_map/all_gather | solution.py:81
  7.9 94.5 %all-gather.7.cloned.1.call-start = ((), (), s32[]{:S(2)}) async-start(), calls=%async_computation | async-start | bytes 4456448 | tf_op jit(solution)/shard_map/all_gather | solution.py:80
  8.7 182.9 %all-gather.9.cloned.1.call-start = ((), (), s32[]{:S(2)}) async-start(), calls=%async_computation.1 | async-start | bytes 4456448 | tf_op jit(solution)/shard_map/all_gather | solution.py:93
  9.4 218.7 %all-gather.13.cloned.1.call-start = ((), (), s32[]{:S(2)}) async-start(), calls=%async_computation.3 | async-start | bytes 1114112 | tf_op jit(solution)/shard_map/all_gather | solution.py:82
  10.0 305.7 %all-reduce.3.cloned.1.call-start = ((), (), s32[]{:S(2)}) async-start(), calls=%async_computation.4 | async-start | bytes 1048576
  36.6 6.7 %copy-start.6 = (f32[64]{0:T(128)S(1)}, f32[64]{0:T(128)}, u32[]{:S(2)}) copy-start(f32[64]{0:T(128)} %param.26) | copy-start | bytes 772
  36.6 6.7 %copy-start.8 = (u32[32]{0:T(128)S(1)}, u32[32]{0:T(128)}, u32[]{:S(2)}) copy-start(u32[32]{0:T(128)} %constant.57) | copy-start | bytes 388
  36.6 14.2 %copy-start.2 = (bf16[4,2048]{1,0:T(4,128)(2,1)S(1)}, bf16[4,2048]{1,0:T(4,128)(2,1)}, u32[]{:S(2)}) copy-start(bf16[4,2048]{1,0:T(4,128)(2,1)} %param.18) | copy-start | bytes 49156
  36.6 14.2 %copy-start.3 = (f32[2048]{0:T(1024)S(1)}, f32[2048]{0:T(1024)}, u32[]{:S(2)}) copy-start(f32[2048]{0:T(1024)} %param.24) | copy-start | bytes 24580
  40.7 64.9 %copy-start.7 = (f32[64]{0:T(128)S(1)}, f32[64]{0:T(128)}, u32[]{:S(2)}) copy-start(f32[64]{0:T(128)} %param.25) | copy-start | bytes 772
  52.7 137.9 %copy-start.1 = (bf16[4,1024,256]{1,2,0:T(8,128)(2,1)S(1)}, bf16[4,1024,256]{1,2,0:T(8,128)(2,1)}, u32[]{:S(2)}) copy-start(bf16[4,1024,256]{1,2,0:T(8,128)(2,1)} %copy.28) | copy-start | bytes 6291460
  190.6 4.1 %copy-start.4 = (f32[2048]{0:T(1024)S(1)}, f32[2048]{0:T(1024)}, u32[]{:S(2)}) copy-start(f32[2048]{0:T(1024)} %param.32) | copy-start | bytes 24580
Sparse Core Ops, SparseCore 0:
  10.2 40.6 all-gather.10
  53.0 49.3 all-gather.6
  104.5 50.9 all-gather.8
  157.6 36.2 all-gather.12
  227.7 87.9 all-reduce.2
where the time goes:
time: 324 us
  waiting for transfers between devices  144 us (44%)
  other arithmetic  87 us (27%)
  blocking collectives  42.8 us (13%)
  matrix products  25.7 us (8%)
  between operations  14.6 us (5%)
  local copies, waits for them, and re-layouts  9.35 us (3%)
    unnamed x6, waiting for transfers between devices  88 us
    another operation x2, other arithmetic  82.1 us
    all_gather x1, waiting for transfers between devices, local(): lax.all_gather(w_query, 'ep', axis=0, tiled=True)  49.7 us
    all_gather x1, blocking collectives, local(): lax.all_gather(route_weights(routes, route_logits), 'ep', axis=0, tiled=T...  23.2 us
    all_gather x1, blocking collectives, local(): input_rows = lax.all_gather(expert_in, 'ep', axis=0, tiled=True)  19.6 us
    dot_general x1, matrix products, local(): jnp.dot(hidden, w_down, preferred_element_type=jnp.float32)  8.67 us
    unnamed x23, local copies, waits for them, and re-layouts  7.29 us
  transfers between devices with their start and end apart: 5, of which 3 were waited for; matrix products, arithmetic and copies ran while one was open for 37% of the time, Pallas kernels for 0%

commit v1 on v0

--- a/solution.py
+++ b/solution.py
@@ -9,6 +9,27 @@
 FF = 7168
 EXPERTS = 4
 EPSILON = 1e-06
+
+
+def in_order(parts, dim):
+    parts = jnp.moveaxis(parts, 0, dim)
+    dims = parts.shape
+    return parts.reshape(*dims[:dim], dims[dim] * dims[dim + 1], *dims[dim + 2 :])
+
+
+def doubled(value, axis):
+    size, index = (lax.axis_size(axis), lax.axis_index(axis))
+    parts, apart = (value[None], 1)
+    while apart < size:
+        received = lax.ppermute(parts, axis, [(i, i ^ apart) for i in range(size)])
+        low = index & apart == 0
+        parts = jnp.concatenate([jnp.where(low, parts, received), jnp.where(low, received, parts)])
+        apart *= 2
+    return parts
+
+
+def doubled_up(x, axis, dim):
+    return in_order(doubled(x, axis), dim)
 
 
 def rms_scaled(values, gain):
@@ -98,7 +119,7 @@
     ff_share = w_gate.shape[1]
     my_expert = lax.axis_index("ep") // (FF // ff_share)
     my_gate = lax.dynamic_slice_in_dim(every_gate, my_expert, 1, 1)
-    input_rows = lax.all_gather(expert_in, "ep", axis=0, tiled=True)
+    input_rows = doubled_up(expert_in, "ep", 0)
     gate_value = jnp.dot(input_rows, w_gate, preferred_element_type=jnp.float32)
     up_value = jnp.dot(input_rows, w_up, preferred_element_type=jnp.float32)
     hidden = (jax.nn.silu(gate_value) * up_value * my_gate).astype(jnp.bfloat16)

time: 324 us -> 304 us (0.938)
  blocking collectives: 42.8 us -> 19 us
  waiting for transfers between devices: 144 us -> 148 us
    all_gather x1 -> x0, blocking collectives: 19.6 us -> none  [local(): input_rows = lax.all_gather(expert_in, 'ep', axis=0, tiled=True)]
    ppermute x0 -> x4, waiting for transfers between devices: none -> 14.3 us  [doubled(): received = lax.ppermute(parts, axis, [(i, i ^ apart) for i in range(size)])]
    all_gather x1, waiting for transfers between devices: 6.25 us -> 0.02 us  [local(): lax.all_gather(w_key, 'ep', axis=0, tiled=True)]
    all_gather x1, waiting for transfers between devices: 49.7 us -> 45 us  [local(): lax.all_gather(w_query, 'ep', axis=0, tiled=True)]
    all_gather x1, blocking collectives: 23.2 us -> 19 us  [local(): lax.all_gather(route_weights(routes, route_logits), 'ep', axis=0, tiled=T...]
    unnamed x23 -> x26, local copies, waits for them, and re-layouts: 7.29 us -> 7.23 us
  transfers between devices with their start and end apart: 5 -> 9, of which waited for: 3 -> 5; matrix products, arithmetic and copies ran while one was open for 37% -> 39% of each run, Pallas kernels for 0% -> 0%
where the time goes in v1:
time: 304 us
  waiting for transfers between devices  148 us (49%)
  other arithmetic  86.9 us (29%)
  matrix products  25.8 us (8%)
  blocking collectives  19 us (6%)
  between operations  14.7 us (5%)
  local copies, waits for them, and re-layouts  8.6 us (3%)
    unnamed x6, waiting for transfers between devices  88.6 us
    another operation x2, other arithmetic  82.1 us
    all_gather x1, waiting for transfers between devices, local(): lax.all_gather(w_query, 'ep', axis=0, tiled=True)  45 us
    all_gather x1, blocking collectives, local(): lax.all_gather(route_weights(routes, route_logits), 'ep', axis=0, tiled=T...  19 us
    ppermute x4, waiting for transfers between devices, doubled(): received = lax.ppermute(parts, axis, [(i, i ^ apart) for i in range(size)])  14.3 us
    dot_general x1, matrix products, local(): jnp.dot(hidden, w_down, preferred_element_type=jnp.float32)  8.68 us
    unnamed x26, local copies, waits for them, and re-layouts  7.23 us
    dot_general x3, matrix products, local(): jnp.dot(normed, weight, preferred_element_type=jnp.float32)  6.47 us
  transfers between devices with their start and end apart: 9, of which 5 were waited for; matrix products, arithmetic and copies ran while one was open for 39% of the time, Pallas kernels for 0%

profile of v1, /device:TPU:0, one launch (start us, length us, event | category | flops | bytes accessed | tf_op | source)
XLA Modules:
  0.0 303.7 jit_solution(370979449245480291)
XLA Ops:
  7.2 0.7 all-gather.6.cloned.1.call-update
  8.0 0.7 all-gather.8.cloned.1.call-update
  8.7 0.7 all-gather.10.cloned.1.call-update
  10.0 0.8 fusion.21
  10.9 0.7 iota_compare_fusion
  11.7 4.0 %copy.27 = bf16[4,1024,256]{1,2,0:T(8,128)(2,1)} copy(bf16[4,1024,256]{2,1,0:T(8,128)(2,1)} %param.20) | data formatting | bytes 4194304 | tf_op args[2]
  15.7 2.5 copy.28
  18.3 45.0 %all-gather.6.cloned.1.call-done = bf16[2048,1024]{1,0:T(8,128)(2,1)} async-done(((bf16[128,1024]{1,0:T(8,128)(2,1)}), bf16[2048,1024]{1,0:T(8,128)(2,1)}) %all-gather.6.cloned.1.call-update) | async-done | bytes 4194320 | tf_op jit(solution)/shard_map/all_gather | solution.py:101
  63.3 2.9 fusion.36
  66.6 2.2 fusion.15
  68.9 79.2 %reduce-window.6 = f32[4,4,4,8,128]{4,3,2,1,0:T(8,128)S(1)} reduce-window(f32[4,4,4,8,128]{4,3,2,1,0:T(8,128)S(1)} %reshape.106, f32[]{:T(128)} %constant.20.clone.1), window={size=1x1x1x1x128 pad=0_0x0_0x0_0x0_0x0_127}, to_apply=%region_2.0 | reduce-window | flops 8323072 | bytes 524292 | tf_op jit(solution)/shard_map/reduce-window
  148.3 2.8 reduce-window.9
  151.5 0.9 convolution_convert_fusion
  152.5 3.0 multiply_reduce_fusion
  156.0 19.0 %all-gather = f32[16,4,4]{2,1,0:T(4,128)S(1)} all-gather(f32[1,4,4]{2,1,0:T(4,128)S(1)} %add_bitcast_fusion), channel_id=1, replica_groups=mesh['grp'=2,'ep'=16] {'ep'}, dimensions={0}, use_global_device_ids=true | all-gather | bytes 1088 | tf_op jit(solution)/shard_map/all_gather | solution.py:118
  176.8 2.3 collective-permute-done.1
  179.3 1.5 fusion.37
  181.0 3.2 %collective-permute-done.2 = bf16[4,4,2048]{2,1,0:T(4,128)(2,1)S(1)} collective-permute-done((bf16[4,4,2048]{2,1,0:T(4,128)(2,1)S(1)}, bf16[4,4,2048]{2,1,0:T(4,128)(2,1)S(1)}, u32[]{:S(2)}, u32[]{:S(2)}) %collective-permute-start.2) | collective-permute-done | bytes 65568 | tf_op jit(solution)/shard_map/ppermute | solution.py:24
  184.6 8.8 %collective-permute-done.3 = bf16[8,4,2048]{2,1,0:T(4,128)(2,1)S(1)} collective-permute-done((bf16[8,4,2048]{2,1,0:T(4,128)(2,1)S(1)}, bf16[8,4,2048]{2,1,0:T(4,128)(2,1)S(1)}, u32[]{:S(2)}, u32[]{:S(2)}) %collective-permute-start.3) | collective-permute-done | bytes 131104 | tf_op jit(solution)/shard_map/ppermute | solution.py:24
  193.8 4.5 %fusion.38 = f32[64,1792]{1,0:T(8,128)S(1)} fusion(bf16[64,2048]{1,0:T(8,128)(2,1)S(1)} %reshape.109, bf16[2048,1792]{1,0:T(8,128)(2,1)} %param.33), kind=kOutput, calls=%fused_computation.74 | convolution fusion | flops 469762048 | bytes 8060928 | tf_op jit(solution)/shard_map/dot_general | solution.py:123
  198.3 8.7 %fusion.3 = f32[64,2048]{1,0:T(8,128)} fusion(bf16[1792,2048]{1,0:T(8,128)(2,1)} %param.35, bf16[64,2048]{1,0:T(8,128)(2,1)S(1)} %reshape.109, bf16[2048,1792]{1,0:T(8,128)(2,1)} %param.34, f32[64,1792]{1,0:T(8,128)S(1)} %fusion.38, f32[64]{0:T(128)S(1)} %bitcast.36), kind=kOutput, calls=%fused_computation.8 | convolution fusion | flops 940326912 | bytes 15925504 | tf_op jit(solution)/shard_map/dot_general | solution.py:127
  207.6 2.1 convolution_convert_fusion.1
  209.7 86.0 %all-reduce.3.cloned.1.call-done = f32[64,2048]{1,0:T(8,128)} async-done(((f32[64,2048]{1,0:T(8,128)}), f32[64,2048]{1,0:T(8,128)}) %all-reduce.3.cloned.1.call-update) | async-done | bytes 524304
  295.7 1.5 fusion.24
  (75 shorter events, 5.3 us)
Async XLA Ops:
  7.2 8.5 %copy-start.7 = (f32[16]{0:T(128)S(1)}, f32[16]{0:T(128)}, u32[]{:S(2)}) copy-start(f32[16]{0:T(128)} %param.27) | copy-start | bytes 196
  7.2 8.5 %copy-start = (bf16[4,1024,256]{2,1,0:T(8,128)(2,1)S(1)}, bf16[4,1024,256]{2,1,0:T(8,128)(2,1)}, u32[]{:S(2)}) copy-start(bf16[4,1024,256]{2,1,0:T(8,128)(2,1)} %param.21) | copy-start | bytes 6291460
  7.2 56.1 %all-gather.6.cloned.1.call-start = ((), (), s32[]{:S(2)}) async-start(), calls=%async_computation | async-start | bytes 4456448 | tf_op jit(solution)/shard_map/all_gather | solution.py:101
  7.9 144.6 %all-gather.8.cloned.1.call-start = ((), (), s32[]{:S(2)}) async-start(), calls=%async_computation.1 | async-start | bytes 4456448 | tf_op jit(solution)/shard_map/all_gather | solution.py:114
  8.7 170.6 %all-gather.10.cloned.1.call-start = ((), (), s32[]{:S(2)}) async-start(), calls=%async_computation.2 | async-start | bytes 1114112 | tf_op jit(solution)/shard_map/all_gather | solution.py:102
  9.4 198.2 %all-gather.12.cloned.1.call-start = ((), (), s32[]{:S(2)}) async-start(), calls=%async_computation.3 | async-start | bytes 1114112 | tf_op jit(solution)/shard_map/all_gather | solution.py:103
  10.0 285.7 %all-reduce.3.cloned.1.call-start = ((), (), s32[]{:S(2)}) async-start(), calls=%async_computation.4 | async-start | bytes 1048576
  11.6 6.6 %copy-start.5 = (s32[4,2]{0,1:T(2,128)S(1)}, s32[4,2]{0,1:T(2,128)}, u32[]{:S(2)}) copy-start(s32[4,2]{0,1:T(2,128)} %param.22) | copy-start | bytes 100
  11.6 6.6 %copy-start.6 = (f32[4,2]{0,1:T(2,128)S(1)}, f32[4,2]{0,1:T(2,128)}, u32[]{:S(2)}) copy-start(f32[4,2]{0,1:T(2,128)} %param.23) | copy-start | bytes 100
  11.6 51.7 %copy-start.2 = (bf16[4,2048]{1,0:T(4,128)(2,1)S(1)}, bf16[4,2048]{1,0:T(4,128)(2,1)}, u32[]{:S(2)}) copy-start(bf16[4,2048]{1,0:T(4,128)(2,1)} %param.18) | copy-start | bytes 49156
  11.6 51.6 %copy-start.3 = (f32[2048]{0:T(1024)S(1)}, f32[2048]{0:T(1024)}, u32[]{:S(2)}) copy-start(f32[2048]{0:T(1024)} %param.24) | copy-start | bytes 24580
  15.7 50.8 %copy-start.9 = (f32[64]{0:T(128)S(1)}, f32[64]{0:T(128)}, u32[]{:S(2)}) copy-start(f32[64]{0:T(128)} %param.25) | copy-start | bytes 772
  18.3 133.2 %copy-start.1 = (bf16[4,1024,256]{1,2,0:T(8,128)(2,1)S(1)}, bf16[4,1024,256]{1,2,0:T(8,128)(2,1)}, u32[]{:S(2)}) copy-start(bf16[4,1024,256]{1,2,0:T(8,128)(2,1)} %copy.28) | copy-start | bytes 6291460
  151.5 4.1 %copy-start.4 = (f32[2048]{0:T(1024)S(1)}, f32[2048]{0:T(1024)}, u32[]{:S(2)}) copy-start(f32[2048]{0:T(1024)} %param.32) | copy-start | bytes 24580
  151.5 24.0 %copy-start.8 = (f32[64]{0:T(128)S(1)}, f32[64]{0:T(128)}, u32[]{:S(2)}) copy-start(f32[64]{0:T(128)} %param.26) | copy-start | bytes 772
  151.5 24.1 %copy-start.10 = (u32[32]{0:T(128)S(1)}, u32[32]{0:T(128)}, u32[]{:S(2)}) copy-start(u32[32]{0:T(128)} %constant.61) | copy-start | bytes 388
  155.6 19.3 %collective-permute-start = (bf16[1,4,2048]{2,1,0:T(4,128)(2,1)S(1)}, bf16[1,4,2048]{2,1,0:T(4,128)(2,1)S(1)}, u32[]{:S(2)}, u32[]{:S(2)}) collective-permute-start(bf16[1,4,2048]{2,1,0:T(4,128)(2,1)S(1)} %fusion.25), channel_id=1, source_target_pairs={{0,1},{1,0},{2,3},{3,2},{4,5},{5,4},{6,7},{7,6},{8,9},{9,8},{10,11... | collective-permute-start | bytes 49160 | tf_op jit(solution)/shard_map/ppermute | solution.py:24
  175.1 4.0 %collective-permute-start.1 = (bf16[2,4,2048]{2,1,0:T(4,128)(2,1)S(1)}, bf16[2,4,2048]{2,1,0:T(4,128)(2,1)S(1)}, u32[]{:S(2)}, u32[]{:S(2)}) collective-permute-start(bf16[2,4,2048]{2,1,0:T(4,128)(2,1)S(1)} %pad_maximum_fusion.3), channel_id=1, source_target_pairs={{0,2},{1,3},{2,0},{3,1},{4,6},{5,7},{6,4},{7,5},{8,10},{9,11},{10,... | collective-permute-start | bytes 98312 | tf_op jit(solution)/shard_map/ppermute | solution.py:24
  179.2 5.0 %collective-permute-start.2 = (bf16[4,4,2048]{2,1,0:T(4,128)(2,1)S(1)}, bf16[4,4,2048]{2,1,0:T(4,128)(2,1)S(1)}, u32[]{:S(2)}, u32[]{:S(2)}) collective-permute-start(bf16[4,4,2048]{2,1,0:T(4,128)(2,1)S(1)} %pad_maximum_fusion.2), channel_id=1, source_target_pairs={{0,4},{1,5},{2,6},{3,7},{4,0},{5,1},{6,2},{7,3},{8,12},{9,13},{10,... | collective-permute-start | bytes 196616 | tf_op jit(solution)/shard_map/ppermute | solution.py:24
  184.4 9.1 %collective-permute-start.3 = (bf16[8,4,2048]{2,1,0:T(4,128)(2,1)S(1)}, bf16[8,4,2048]{2,1,0:T(4,128)(2,1)S(1)}, u32[]{:S(2)}, u32[]{:S(2)}) collective-permute-start(bf16[8,4,2048]{2,1,0:T(4,128)(2,1)S(1)} %pad_maximum_fusion.1), channel_id=1, source_target_pairs={{0,8},{1,9},{2,10},{3,11},{4,12},{5,13},{6,14},{7,15},{8,0},{9,1},... | collective-permute-start | bytes 393224 | tf_op jit(solution)/shard_map/ppermute | solution.py:24
Sparse Core Ops, SparseCore 0:
  10.2 53.0 all-gather.5
  65.4 50.9 all-gather.7
  118.6 36.2 all-gather.9
  156.9 38.1 all-gather.11
  207.1 88.5 all-reduce.2
